TPU v7x, 32 devices: a whole 2x2x4 slice. The times are simulated.
32 devices in a mesh: sp: 8 (over z, x), tp: 4 (over y, core).
Axes of the slice: x: 2, y: 2, z: 4, core: 2. Of those that a mesh axis runs over, the one named last changes fastest.
Arguments:
- tokens: bfloat16 [2048, 2048], P('sp'), may hold values from -6 to 6
- documents: int32 [2048], P('sp'), may hold values from 0 to 3, never falling along the last dimension, each value on 1 to 1024 neighbouring positions
- norm_gain: float32 [1, 2048], replicated, may hold values from 0.1 to 1.9
- w_query: bfloat16 [1, 2048, 2048], P(None, 'sp', 'tp'), may hold values from -0.125 to 0.125
- w_key: bfloat16 [1, 2048, 2048], P(None, 'sp', 'tp'), may hold values from -0.125 to 0.125
- w_value: bfloat16 [1, 2048, 2048], P(None, 'sp', 'tp'), may hold values from -0.125 to 0.125
- w_out: bfloat16 [1, 2048, 2048], P(None, None, 'sp'), may hold values from -0.59765625 to 0.59765625
- rel_bias: float32 [1, 32, 257], P(None, 'tp'), may hold values from -8 to 240
Outputs:
- mixed: bfloat16 [2048, 2048], P('sp')
Inputs may be any that keep to these rules, and one draw needn't show every extreme that they name: `documents`: document numbers never fall along the sequence; a document has 1 to 1024 positions.
All inputs are finite; a program needn't handle non-finite values.
Results may differ from a plain program's by a relative error of at most 0.007.
Values may be sent and summed in bfloat16 or wider, within the bound.
A program may use at most 128 MiB of HBM per device.

v0:
```python
import jax
import jax.numpy as jnp
from jax import lax
from jax.sharding import PartitionSpec as P

HEAD_DIM = 64
SEG = 64
LEFT = 4
REL_CLIP = 128
EPS = 1e-06


def passed_along(x, axis, by):
    length = lax.axis_size(axis)
    pairs = [(i, i + by) for i in range(length) if 0 <= i + by < length]
    return lax.ppermute(x, axis, pairs)


def banded_bias(bias_table, query_rows, key_rows, reach_rows):
    span_len = query_rows + key_rows - 1
    steps_back = jnp.arange(span_len, dtype=jnp.int32) - (key_rows - 1) + reach_rows
    lookup = jnp.clip(steps_back, -REL_CLIP, REL_CLIP) + REL_CLIP
    bias_line = jnp.take(bias_table, lookup, axis=1)
    reversed_line = bias_line[:, ::-1]
    repeated = jnp.tile(reversed_line, (1, query_rows))
    skewed = repeated[:, query_rows - 1 : query_rows - 1 + query_rows * (span_len - 1)]
    skewed = skewed.reshape(bias_table.shape[0], query_rows, span_len - 1)
    return skewed[:, :, :key_rows]


def attend(queries, keys_all, values_all, query_pos, key_pos, query_doc, key_doc, bias_table):
    query_rows = queries.shape[0]
    key_rows = keys_all.shape[0]
    reach_rows = key_rows - query_rows
    scores = jnp.einsum(
        "qhe,khe->hqk", queries, keys_all, preferred_element_type=jnp.float32
    ) * HEAD_DIM ** (-0.5)
    scores = scores + banded_bias(bias_table, query_rows, key_rows, reach_rows)
    query_seg = query_pos // SEG
    key_seg = key_pos // SEG
    allowed = (
        (key_pos[None, :] >= 0)
        & (key_seg[None, :] <= query_seg[:, None])
        & (key_seg[None, :] >= query_seg[:, None] - LEFT)
        & (key_doc[None, :] == query_doc[:, None])
    )
    scores = jnp.where(allowed[None], scores, -1e30)
    peak = jnp.max(scores, axis=-1, keepdims=True)
    raised = jnp.exp(scores - peak)
    weights_bf = (raised / jnp.sum(raised, axis=-1, keepdims=True)).astype(jnp.bfloat16)
    return jnp.einsum(
        "hqk,khe->qhe", weights_bf, values_all, preferred_element_type=jnp.float32
    ).astype(jnp.bfloat16)


def body(tokens, documents, norm_gain, w_query, w_key, w_value, w_out, rel_bias):
    local_rows = tokens.shape[0]
    reach_rows = LEFT * SEG
    width_local = w_query.shape[2]
    heads_local = width_local // HEAD_DIM
    offset = lax.axis_index("sp") * local_rows
    query_pos = offset + jnp.arange(local_rows, dtype=jnp.int32)
    key_pos = offset - reach_rows + jnp.arange(reach_rows + local_rows, dtype=jnp.int32)
    widened = tokens.astype(jnp.float32)
    normed = (
        widened
        * lax.rsqrt(jnp.mean(widened * widened, axis=-1, keepdims=True) + EPS)
        * norm_gain[0]
    ).astype(jnp.bfloat16)
    query_sum = jnp.dot(
        normed,
        lax.all_gather(w_query[0], "sp", axis=0, tiled=True),
        preferred_element_type=jnp.float32,
    )
    key_sum = jnp.dot(
        normed,
        lax.all_gather(w_key[0], "sp", axis=0, tiled=True),
        preferred_element_type=jnp.float32,
    )
    value_sum = jnp.dot(
        normed,
        lax.all_gather(w_value[0], "sp", axis=0, tiled=True),
        preferred_element_type=jnp.float32,
    )
    queries = query_sum.astype(jnp.bfloat16)
    keys_own = key_sum.astype(jnp.bfloat16)
    values_own = value_sum.astype(jnp.bfloat16)
    prior_keys, prior_values, prior_docs = passed_along((keys_own, values_own, documents), "sp", 1)
    keys_all = jnp.concatenate([prior_keys, keys_own], axis=0)
    values_all = jnp.concatenate([prior_values, values_own], axis=0)
    key_doc = jnp.concatenate([prior_docs, documents], axis=0)
    attended = attend(
        queries.reshape(local_rows, heads_local, HEAD_DIM),
        keys_all.reshape(reach_rows + local_rows, heads_local, HEAD_DIM),
        values_all.reshape(reach_rows + local_rows, heads_local, HEAD_DIM),
        query_pos,
        key_pos,
        documents,
        key_doc,
        rel_bias[0],
    ).reshape(local_rows, width_local)
    all_heads = lax.all_gather(attended, "tp", axis=1, tiled=True)
    return (
        widened
        + jnp.dot(
            all_heads,
            lax.all_gather(w_out[0], "sp", axis=1, tiled=True),
            preferred_element_type=jnp.float32,
        )
    ).astype(jnp.bfloat16)


def solution(mesh):
    in_specs = (
        P("sp", None),
        P("sp"),
        P(),
        P(None, "sp", "tp"),
        P(None, "sp", "tp"),
        P(None, "sp", "tp"),
        P(None, None, "sp"),
        P(None, "tp", None),
    )
    out_specs = P("sp", None)
    return jax.shard_map(body, mesh=mesh, in_specs=in_specs, out_specs=out_specs, check_vma=False)
```

profile of v0, /device:TPU:0, one launch (start us, length us, event | category | flops | bytes accessed | tf_op | source)
XLA Modules:
  0.0 332.9 jit_solution(15047874739899325037)
XLA Ops:
  6.5 0.0 all-gather.12.cloned.1.call-start
  6.5 0.7 all-gather.12.cloned.1.call-update
  7.3 0.0 all-gather.16.cloned.1.call-start
  7.3 0.7 all-gather.16.cloned.1.call-update
  8.0 0.0 all-gather.14.cloned.1.call-start
  8.1 0.7 all-gather.14.cloned.1.call-update
  8.7 0.0 all-gather.10.cloned.1.call-start
  8.8 4.9 %collective-permute-start.1 = (s32[256]{0:T(256)}, s32[256]{0:T(256)S(1)}, u32[]{:S(2)}, u32[]{:S(2)}) collective-permute-start(s32[256]{0:T(256)} %param.9), channel_id=1, source_target_pairs={{0,4},{4,8},{8,12},{12,16},{16,20},{20,24},{24,28},{1,5},{5,9},{9,... | collective-permute-start | bytes 3080 | tf_op jit(solution)/shard_map/ppermute | solution.py:16
  13.7 0.8 copy.17
  14.6 1.6 gather_fusion
  16.2 1.5 fusion.9
  17.7 0.2 select_bitcast_fusion
  17.9 0.5 rev.3
  18.4 0.1 copy.18
  18.5 3.1 tile.4
  21.6 8.7 %tile.10 = f32[8,196352]{1,0:T(8,128)} reshape(f32[8,256,767]{2,1,0:T(8,128)} %tile.4) | data formatting | bytes 12566528 | tf_op jit(solution)/shard_map/tile | solution.py:25
  30.3 5.4 %slice.10 = f32[8,196096]{1,0:T(8,128)} slice(f32[8,196352]{1,0:T(8,128)} %tile.10), slice={[0:8], [255:196351]} | slice | bytes 12550144 | tf_op jit(solution)/shard_map/slice | solution.py:26
  35.7 0.0 copy-start.2
  35.7 0.0 copy-start.1
  35.7 0.0 copy-start.3
  35.7 12.4 %reshape.203 = f32[8,256,766]{2,1,0:T(8,128)} reshape(f32[8,196096]{1,0:T(8,128)} %slice.10) | data formatting | bytes 12550144 | tf_op jit(solution)/shard_map/reshape | solution.py:27
  48.1 0.0 collective-permute-done.1
  48.1 0.0 copy-done.2
  48.1 0.3 compare_and_fusion
  48.4 12.9 %all-gather.12.cloned.1.call-done = bf16[1,2048,512]{2,1,0:T(8,128)(2,1)} async-done(((bf16[1,256,512]{2,1,0:T(8,128)(2,1)}), bf16[1,2048,512]{2,1,0:T(8,128)(2,1)}) %all-gather.12.cloned.1.call-update) | async-done | bytes 2097168 | tf_op jit(solution)/shard_map/all_gather | solution.py:82
  61.3 0.0 copy-done.1
  61.3 0.0 copy-done.3
  61.3 2.3 fusion.20
  63.7 2.5 collective-permute-start
  66.1 45.1 %all-gather.16.cloned.1.call-done = bf16[1,2048,512]{2,1,0:T(8,128)(2,1)} async-done(((bf16[1,256,512]{2,1,0:T(8,128)(2,1)}), bf16[1,2048,512]{2,1,0:T(8,128)(2,1)}) %all-gather.16.cloned.1.call-update) | async-done | bytes 2097168 | tf_op jit(solution)/shard_map/all_gather | solution.py:77
  111.2 2.3 fusion.26
  113.5 2.7 collective-permute-start.2
  116.3 44.9 %all-gather.14.cloned.1.call-done = bf16[1,2048,512]{2,1,0:T(8,128)(2,1)} async-done(((bf16[1,256,512]{2,1,0:T(8,128)(2,1)}), bf16[1,2048,512]{2,1,0:T(8,128)(2,1)}) %all-gather.14.cloned.1.call-update) | async-done | bytes 2097168 | tf_op jit(solution)/shard_map/all_gather | solution.py:72
  161.1 2.3 fusion.23
  163.5 0.1 copy.15
  163.6 0.0 collective-permute-done
  163.7 0.2 copy.14
  163.9 0.0 collective-permute-done.2
  163.9 0.2 copy.16
  164.1 3.1 fusion.3
  167.2 0.0 copy-start
  167.2 1.7 fusion.41
  169.0 0.2 copy-done
  169.2 8.0 %fusion.19 = bf16[8,64,256]{2,1,0:T(8,128)(2,1)} fusion(bf16[512,8,64]{0,2,1:T(8,128)(2,1)S(1)} %bitcast.41, f32[8,256]{1,0:T(8,128)S(1)} %fusion.41, f32[8,256,512]{2,1,0:T(8,128)} %copy-done), kind=kOutput, calls=%fused_computation.22 | convolution fusion | flops 137497088 | bytes 4988928 | tf_op jit(solution)/shard_map/hqk,khe->qhe/dot_general | solution.py:51
  177.1 0.0 all-gather.10.cloned.1.call-update
  177.1 0.0 all-gather.18.cloned.1.call-start
  177.2 0.5 all-gather.18.cloned.1.call-update
  177.7 14.8 %all-gather.10.cloned.1.call-done = bf16[256,2048]{0,1:T(8,128)(2,1)} async-done(((bf16[256,512]{0,1:T(8,128)(2,1)}), bf16[256,2048]{0,1:T(8,128)(2,1)}) %all-gather.10.cloned.1.call-update) | async-done | bytes 1048592 | tf_op jit(solution)/shard_map/all_gather | solution.py:102
  192.5 126.8 %all-gather.18.cloned.1.call-done = bf16[1,2048,2048]{2,1,0:T(8,128)(2,1)} async-done(((bf16[1,2048,256]{2,1,0:T(8,128)(2,1)}), bf16[1,2048,2048]{2,1,0:T(8,128)(2,1)}) %all-gather.18.cloned.1.call-update) | async-done | bytes 8388624 | tf_op jit(solution)/shard_map/all_gather | solution.py:107
  319.4 7.0 %fusion.6 = bf16[256,2048]{1,0:T(8,128)(2,1)} fusion(bf16[256,2048]{0,1:T(8,128)(2,1)} %all-gather.10.cloned.1.call-done, bf16[1,2048,2048]{2,1,0:T(8,128)(2,1)} %all-gather.18.cloned.1.call-done, bf16[256,2048]{1,0:T(8,128)(2,1)S(1)} %copy-done.1), kind=kOutput, calls=%fused_computation.11 | convolution fusion | flops 2149056512 | bytes 11534336 | tf_op jit(solution)/shard_map/dot_general | solution.py:105
  (10 shorter events, 0.2 us)
Async XLA Ops:
  6.5 54.8 %all-gather.12.cloned.1.call-start = ((), (), s32[]{:S(2)}) async-start(), calls=%async_computation.1 | async-start | bytes 2359296 | tf_op jit(solution)/shard_map/all_gather | solution.py:82
  7.3 103.9 %all-gather.16.cloned.1.call-start = ((), (), s32[]{:S(2)}) async-start(), calls=%async_computation.3 | async-start | bytes 2359296 | tf_op jit(solution)/shard_map/all_gather | solution.py:77
  8.0 153.1 %all-gather.14.cloned.1.call-start = ((), (), s32[]{:S(2)}) async-start(), calls=%async_computation.2 | async-start | bytes 2359296 | tf_op jit(solution)/shard_map/all_gather | solution.py:72
  8.7 183.8 %all-gather.10.cloned.1.call-start = ((), (), s32[]{:S(2)}) async-start(), calls=%async_computation | async-start | bytes 1310720 | tf_op jit(solution)/shard_map/all_gather | solution.py:102
  8.8 39.3 %collective-permute-start.1 = (s32[256]{0:T(256)}, s32[256]{0:T(256)S(1)}, u32[]{:S(2)}, u32[]{:S(2)}) collective-permute-start(s32[256]{0:T(256)} %param.9), channel_id=1, source_target_pairs={{0,4},{4,8},{8,12},{12,16},{16,20},{20,24},{24,28},{1,5},{5,9},{9,... | collective-permute-start | bytes 3080 | tf_op jit(solution)/shard_map/ppermute | solution.py:16
  35.7 12.4 %copy-start.2 = (s32[256]{0:T(256)S(1)}, s32[256]{0:T(256)}, u32[]{:S(2)}) copy-start(s32[256]{0:T(256)} %param.9) | copy-start | bytes 3076
  35.7 25.6 %copy-start.1 = (bf16[256,2048]{1,0:T(8,128)(2,1)S(1)}, bf16[256,2048]{1,0:T(8,128)(2,1)}, u32[]{:S(2)}) copy-start(bf16[256,2048]{1,0:T(8,128)(2,1)} %param.8) | copy-start | bytes 3145732
  35.7 25.6 %copy-start.3 = (f32[1,2048]{1,0:T(1,128)S(1)}, f32[1,2048]{1,0:T(1,128)}, u32[]{:S(2)}) copy-start(f32[1,2048]{1,0:T(1,128)} %param.10) | copy-start | bytes 24580
  63.7 100.0 %collective-permute-start = (bf16[256,512]{1,0:T(8,128)(2,1)S(1)}, bf16[256,512]{1,0:T(8,128)(2,1)S(1)}, u32[]{:S(2)}, u32[]{:S(2)}) collective-permute-start(bf16[256,512]{1,0:T(8,128)(2,1)S(1)} %fusion.20), channel_id=1, source_target_pairs={{0,4},{4,8},{8,12},{12,16},{16,20},{20,24},{24,28},{1,5},{5,9},{9,... | collective-permute-start | bytes 786440 | tf_op jit(solution)/shard_map/ppermute | solution.py:16
  113.5 50.3 %collective-permute-start.2 = (bf16[256,512]{1,0:T(8,128)(2,1)S(1)}, bf16[256,512]{1,0:T(8,128)(2,1)S(1)}, u32[]{:S(2)}, u32[]{:S(2)}) collective-permute-start(bf16[256,512]{1,0:T(8,128)(2,1)S(1)} %fusion.26), channel_id=1, source_target_pairs={{0,4},{4,8},{8,12},{12,16},{16,20},{20,24},{24,28},{1,5},{5,9},{9,... | collective-permute-start | bytes 786440 | tf_op jit(solution)/shard_map/ppermute | solution.py:16
  167.2 1.9 copy-start
  177.1 142.2 %all-gather.18.cloned.1.call-start = ((), (), s32[]{:S(2)}) async-start(), calls=%async_computation.4 | async-start | bytes 9437184 | tf_op jit(solution)/shard_map/all_gather | solution.py:107
Sparse Core Ops, SparseCore 0:
  9.5 51.7 all-gather.11
  63.4 47.7 all-gather.15
  113.3 47.7 all-gather.13
  177.3 15.2 all-gather.9
  194.4 124.9 all-gather.17
where the time goes:
time: 333 us
  waiting for transfers between devices  247 us (74%)
  local copies, waits for them, and re-layouts  33.3 us (10%)
  matrix products  25.1 us (8%)
  between operations  13.3 us (4%)
  starting transfers between devices  10.2 us (3%)
  other arithmetic  3.84 us (1%)
    all_gather x1, waiting for transfers between devices, body(): lax.all_gather(w_out[0], 'sp', axis=1, tiled=True)  127 us
    all_gather x1, waiting for transfers between devices, body(): lax.all_gather(w_key[0], 'sp', axis=0, tiled=True)  45.1 us
    all_gather x1, waiting for transfers between devices, body(): lax.all_gather(w_query[0], 'sp', axis=0, tiled=True)  44.9 us
    all_gather x1, waiting for transfers between devices, body(): all_heads = lax.all_gather(attended, 'tp', axis=1, tiled=True)  14.8 us
    all_gather x1, waiting for transfers between devices, body(): lax.all_gather(w_value[0], 'sp', axis=0, tiled=True)  12.9 us
    reshape x1, local copies, waits for them, and re-layouts, banded_bias(): skewed = skewed.reshape(bias_table.shape[0], query_rows, span_len - 1)  12.4 us
    another operation x2, local copies, waits for them, and re-layouts, banded_bias(): repeated = jnp.tile(reversed_line, (1, query_rows))  11.8 us
    ppermute x3, starting transfers between devices, passed_along(): return lax.ppermute(x, axis, pairs)  10 us
  transfers between devices with their start and end apart: 8, of which 5 were waited for; matrix products, arithmetic and copies ran while one was open for 13% of the time, Pallas kernels for 0%

commit v1 on v0

--- a/solution.py
+++ b/solution.py
@@ -2,6 +2,7 @@
 import jax.numpy as jnp
 from jax import lax
 from jax.sharding import PartitionSpec as P
+from jax.lax import all_to_all, axis_size
 
 HEAD_DIM = 64
 SEG = 64
@@ -67,10 +68,16 @@
         * lax.rsqrt(jnp.mean(widened * widened, axis=-1, keepdims=True) + EPS)
         * norm_gain[0]
     ).astype(jnp.bfloat16)
+
+    def point_sums_all_on_mesh(in_array):
+        grid = []
+        for _ in range(axis_size("sp")):
+            grid.append(in_array)
+        heard = jnp.concatenate(all_to_all(jnp.stack(grid, 0), "sp", 0, 0), 0)
+        return heard
+
     query_sum = jnp.dot(
-        normed,
-        lax.all_gather(w_query[0], "sp", axis=0, tiled=True),
-        preferred_element_type=jnp.float32,
+        normed, point_sums_all_on_mesh(w_query[0]), preferred_element_type=jnp.float32
     )
     key_sum = jnp.dot(
         normed,

time: 333 us -> 327 us (0.982)
  waiting for transfers between devices: 247 us -> 225 us
  starting transfers between devices: 10.2 us -> 17.2 us
  local copies, waits for them, and re-layouts: 33.3 us -> 38.3 us
  other arithmetic: 3.84 us -> 7.44 us
    all_gather x1 -> x0, waiting for transfers between devices: 44.9 us -> none  [body(): lax.all_gather(w_query[0], 'sp', axis=0, tiled=True)]
    all_gather x1, waiting for transfers between devices: 12.9 us -> 31.9 us  [body(): lax.all_gather(w_value[0], 'sp', axis=0, tiled=True)]
    all_to_all x0 -> x1, starting transfers between devices: none -> 7.41 us  [point_sums_all_on_mesh(): heard = jnp.concatenate(all_to_all(jnp.stack(grid, 0), 'sp', 0, 0), 0)]
    all_gather x1, waiting for transfers between devices: 14.8 us -> 18.7 us  [body(): all_heads = lax.all_gather(attended, 'tp', axis=1, tiled=True)]
  transfers between devices with their start and end apart: 8 -> 8, of which waited for: 5 -> 5; matrix products, arithmetic and copies ran while one was open for 13% -> 15% of each run, Pallas kernels for 0% -> 0%
where the time goes in v1:
time: 327 us; the launch traced here: 326 us
  waiting for transfers between devices  225 us (69%)
  local copies, waits for them, and re-layouts  38.3 us (12%)
  matrix products  24.9 us (8%)
  starting transfers between devices  17.2 us (5%)
  between operations  13.3 us (4%)
  other arithmetic  7.44 us (2%)
    all_gather x1, waiting for transfers between devices, body(): lax.all_gather(w_out[0], 'sp', axis=1, tiled=True)  127 us
    all_gather x1, waiting for transfers between devices, body(): lax.all_gather(w_key[0], 'sp', axis=0, tiled=True)  44.3 us
    all_gather x1, waiting for transfers between devices, body(): lax.all_gather(w_value[0], 'sp', axis=0, tiled=True)  31.9 us
    all_gather x1, waiting for transfers between devices, body(): all_heads = lax.all_gather(attended, 'tp', axis=1, tiled=True)  18.7 us
    reshape x1, local copies, waits for them, and re-layouts, banded_bias(): skewed = skewed.reshape(bias_table.shape[0], query_rows, span_len - 1)  12.3 us
    another operation x2, local copies, waits for them, and re-layouts, banded_bias(): repeated = jnp.tile(reversed_line, (1, query_rows))  11.8 us
    ppermute x3, starting transfers between devices, passed_along(): return lax.ppermute(x, axis, pairs)  9.7 us
    dot_general x1, matrix products, attend(): jnp.einsum('hqk,khe->qhe', weights_bf, values_all, preferred_element_type...  7.95 us
  transfers between devices with their start and end apart: 8, of which 5 were waited for; matrix products, arithmetic and copies ran while one was open for 15% of the time, Pallas kernels for 0%

profile of v1, /device:TPU:0, one launch (start us, length us, event | category | flops | bytes accessed | tf_op | source)
XLA Modules:
  0.0 326.1 jit_solution(3843189563401212288)
XLA Ops:
  6.5 0.0 all-gather.10.cloned.1.call-start
  6.5 0.7 all-gather.10.cloned.1.call-update
  7.3 0.0 all-gather.12.cloned.1.call-start
  7.3 0.7 all-gather.12.cloned.1.call-update
  8.0 2.5 stack.3
  10.5 0.0 copy-start.3
  10.5 0.0 copy-start.2
  10.5 0.0 copy-start.1
  10.5 7.4 %all-to-all-start = ((bf16[8,256,512]{2,1,0:T(8,128)(2,1)}), bf16[8,256,512]{2,1,0:T(8,128)(2,1)S(1)}, u32[]{:S(2)}, u32[]{:S(2)}) async-start(bf16[8,256,512]{2,1,0:T(8,128)(2,1)} %stack.3), calls=%async_computation | async-start | bytes 4194304 | tf_op jit(solution)/shard_map/all_to_all | solution.py:76
  17.9 0.0 all-gather.8.cloned.1.call-start
  17.9 0.0 copy-done.3
  17.9 4.4 %collective-permute-start.1 = (s32[256]{0:T(256)S(1)}, s32[256]{0:T(256)}, u32[]{:S(2)}, u32[]{:S(2)}) collective-permute-start(s32[256]{0:T(256)S(1)} %copy-done.3), channel_id=1, source_target_pairs={{0,4},{4,8},{8,12},{12,16},{16,20},{20,24},{24,28},{1,5},{5,9},{9,... | collective-permute-start | bytes 3080 | tf_op jit(solution)/shard_map/ppermute | solution.py:17
  22.4 0.0 copy-done.2
  22.4 0.1 copy.17
  22.5 2.3 gather_fusion
  24.9 0.0 copy-done.1
  24.9 0.3 fusion.9
  25.2 0.6 add_rsqrt_fusion
  25.8 1.2 select_bitcast_fusion
  26.9 0.5 fusion.30
  27.5 2.0 rev.3
  29.5 1.1 copy.18
  30.6 3.1 tile.4
  33.7 8.7 %tile.10 = f32[8,196352]{1,0:T(8,128)} reshape(f32[8,256,767]{2,1,0:T(8,128)} %tile.4) | data formatting | bytes 12566528 | tf_op jit(solution)/shard_map/tile | solution.py:26
  42.4 5.4 %slice.10 = f32[8,196096]{1,0:T(8,128)} slice(f32[8,196352]{1,0:T(8,128)} %tile.10), slice={[0:8], [255:196351]} | slice | bytes 12550144 | tf_op jit(solution)/shard_map/slice | solution.py:27
  47.8 0.0 copy-start.6
  47.8 0.0 copy-start.4
  47.8 0.0 copy-start.7
  47.8 12.3 %reshape.208 = f32[8,256,766]{2,1,0:T(8,128)} reshape(f32[8,196096]{1,0:T(8,128)} %slice.10) | data formatting | bytes 12550144 | tf_op jit(solution)/shard_map/reshape | solution.py:28
  60.1 0.0 collective-permute-done.1
  60.1 0.6 pad_add_fusion
  60.8 0.0 copy-done.6
  60.8 0.3 compare_and_fusion
  61.0 31.9 %all-gather.10.cloned.1.call-done = bf16[1,2048,512]{2,1,0:T(8,128)(2,1)} async-done(((bf16[1,256,512]{2,1,0:T(8,128)(2,1)}), bf16[1,2048,512]{2,1,0:T(8,128)(2,1)}) %all-gather.10.cloned.1.call-update) | async-done | bytes 2097168 | tf_op jit(solution)/shard_map/all_gather | solution.py:89
  93.0 0.0 copy-done.4
  93.0 0.0 copy-done.7
  93.0 3.0 fusion.18
  96.0 0.0 copy-start.5
  96.0 2.1 collective-permute-start
  98.1 44.3 %all-gather.12.cloned.1.call-done = bf16[1,2048,512]{2,1,0:T(8,128)(2,1)} async-done(((bf16[1,256,512]{2,1,0:T(8,128)(2,1)}), bf16[1,2048,512]{2,1,0:T(8,128)(2,1)}) %all-gather.12.cloned.1.call-update) | async-done | bytes 2097168 | tf_op jit(solution)/shard_map/all_gather | solution.py:84
  142.4 3.1 fusion.21
  145.5 3.2 collective-permute-start.2
  148.6 0.0 all-to-all-done
  148.6 0.0 copy-done.5
  148.6 0.0 copy-done.8
  148.6 0.8 convolution_convert_fusion
  149.4 0.1 copy.15
  149.5 0.0 collective-permute-done
  149.6 1.1 pad_maximum_fusion
  150.6 0.2 copy.14
  150.8 1.3 collective-permute-done.2
  152.1 1.1 pad_maximum_fusion.1
  153.2 0.2 copy.16
  153.4 3.1 fusion.3
  156.5 0.0 copy-start
  156.5 1.7 fusion.36
  158.2 0.2 copy-done
  158.4 8.0 %fusion.17 = bf16[8,64,256]{2,1,0:T(8,128)(2,1)} fusion(bf16[512,8,64]{0,2,1:T(8,128)(2,1)S(1)} %bitcast.40, f32[8,256]{1,0:T(8,128)S(1)} %fusion.36, f32[8,256,512]{2,1,0:T(8,128)} %copy-done), kind=kOutput, calls=%fused_computation.20 | convolution fusion | flops 137497088 | bytes 4988928 | tf_op jit(solution)/shard_map/hqk,khe->qhe/dot_general | solution.py:52
  166.4 0.0 all-gather.8.cloned.1.call-update
  166.4 0.0 all-gather.14.cloned.1.call-start
  166.4 0.5 all-gather.14.cloned.1.call-update
  167.0 18.7 %all-gather.8.cloned.1.call-done = bf16[256,2048]{0,1:T(8,128)(2,1)} async-done(((bf16[256,512]{0,1:T(8,128)(2,1)}), bf16[256,2048]{0,1:T(8,128)(2,1)}) %all-gather.8.cloned.1.call-update) | async-done | bytes 1048592 | tf_op jit(solution)/shard_map/all_gather | solution.py:109
  185.7 126.9 %all-gather.14.cloned.1.call-done = bf16[1,2048,2048]{2,1,0:T(8,128)(2,1)} async-done(((bf16[1,2048,256]{2,1,0:T(8,128)(2,1)}), bf16[1,2048,2048]{2,1,0:T(8,128)(2,1)}) %all-gather.14.cloned.1.call-update) | async-done | bytes 8388624 | tf_op jit(solution)/shard_map/all_gather | solution.py:114
  312.6 7.0 %fusion.6 = bf16[256,2048]{1,0:T(8,128)(2,1)} fusion(bf16[256,2048]{0,1:T(8,128)(2,1)} %all-gather.8.cloned.1.call-done, bf16[1,2048,2048]{2,1,0:T(8,128)(2,1)} %all-gather.14.cloned.1.call-done, bf16[256,2048]{1,0:T(8,128)(2,1)S(1)} %copy-done.1), kind=kOutput, calls=%fused_computation.11 | convolution fusion | flops 2149056512 | bytes 11534336 | tf_op jit(solution)/shard_map/dot_general | solution.py:112
  (6 shorter events, 0.1 us)
Async XLA Ops:
  6.5 86.4 %all-gather.10.cloned.1.call-start = ((), (), s32[]{:S(2)}) async-start(), calls=%async_computation.2 | async-start | bytes 2359296 | tf_op jit(solution)/shard_map/all_gather | solution.py:89
  7.3 135.2 %all-gather.12.cloned.1.call-start = ((), (), s32[]{:S(2)}) async-start(), calls=%async_computation.3 | async-start | bytes 2359296 | tf_op jit(solution)/shard_map/all_gather | solution.py:84
  10.5 7.5 %copy-start.3 = (s32[256]{0:T(256)S(1)}, s32[256]{0:T(256)}, u32[]{:S(2)}) copy-start(s32[256]{0:T(256)} %param.9) | copy-start | bytes 3076
  10.5 11.9 %copy-start.2 = (f32[1,8,257]{2,1,0:T(8,128)S(1)}, f32[1,8,257]{2,1,0:T(8,128)}, u32[]{:S(2)}) copy-start(f32[1,8,257]{2,1,0:T(8,128)} %param.15) | copy-start | bytes 24676
  10.5 14.4 %copy-start.1 = (bf16[256,2048]{1,0:T(8,128)(2,1)S(1)}, bf16[256,2048]{1,0:T(8,128)(2,1)}, u32[]{:S(2)}) copy-start(bf16[256,2048]{1,0:T(8,128)(2,1)} %param.8) | copy-start | bytes 3145732
  10.5 138.2 %all-to-all-start = ((bf16[8,256,512]{2,1,0:T(8,128)(2,1)}), bf16[8,256,512]{2,1,0:T(8,128)(2,1)S(1)}, u32[]{:S(2)}, u32[]{:S(2)}) async-start(bf16[8,256,512]{2,1,0:T(8,128)(2,1)} %stack.3), calls=%async_computation | async-start | bytes 4194304 | tf_op jit(solution)/shard_map/all_to_all | solution.py:76
  17.9 167.8 %all-gather.8.cloned.1.call-start = ((), (), s32[]{:S(2)}) async-start(), calls=%async_computation.1 | async-start | bytes 1310720 | tf_op jit(solution)/shard_map/all_gather | solution.py:109
  17.9 42.2 %collective-permute-start.1 = (s32[256]{0:T(256)S(1)}, s32[256]{0:T(256)}, u32[]{:S(2)}, u32[]{:S(2)}) collective-permute-start(s32[256]{0:T(256)S(1)} %copy-done.3), channel_id=1, source_target_pairs={{0,4},{4,8},{8,12},{12,16},{16,20},{20,24},{24,28},{1,5},{5,9},{9,... | collective-permute-start | bytes 3080 | tf_op jit(solution)/shard_map/ppermute | solution.py:17
  47.8 13.0 %copy-start.6 = (pred[512]{0:T(512)(128)(4,1)S(1)}, pred[512]{0:T(512)(128)(4,1)}, u32[]{:S(2)}) copy-start(pred[512]{0:T(512)(128)(4,1)} %fusion.30) | copy-start | bytes 1540
  47.8 45.2 %copy-start.4 = (f32[256]{0:T(256)S(1)}, f32[256]{0:T(256)}, u32[]{:S(2)}) copy-start(f32[256]{0:T(256)} %add_rsqrt_fusion) | copy-start | bytes 3076
  47.8 45.2 %copy-start.7 = (f32[1,2048]{1,0:T(1,128)S(1)}, f32[1,2048]{1,0:T(1,128)}, u32[]{:S(2)}) copy-start(f32[1,2048]{1,0:T(1,128)} %param.10) | copy-start | bytes 24580
  96.0 52.6 %copy-start.5 = (f32[256]{0:T(256)S(1)}, f32[256]{0:T(256)}, u32[]{:S(2)}) copy-start(f32[256]{0:T(256)} %add_rsqrt_fusion) | copy-start | bytes 3076
  96.0 52.6 %copy-start.8 = (f32[1,2048]{1,0:T(1,128)S(1)}, f32[1,2048]{1,0:T(1,128)}, u32[]{:S(2)}) copy-start(f32[1,2048]{1,0:T(1,128)} %param.10) | copy-start | bytes 24580
  96.0 53.5 %collective-permute-start = (bf16[256,512]{1,0:T(8,128)(2,1)}, bf16[256,512]{1,0:T(8,128)(2,1)}, u32[]{:S(2)}, u32[]{:S(2)}) collective-permute-start(bf16[256,512]{1,0:T(8,128)(2,1)} %fusion.18), channel_id=1, source_target_pairs={{0,4},{4,8},{8,12},{12,16},{16,20},{20,24},{24,28},{1,5},{5,9},{9,... | collective-permute-start | bytes 786440 | tf_op jit(solution)/shard_map/ppermute | solution.py:17
  145.5 6.6 %collective-permute-start.2 = (bf16[256,512]{1,0:T(8,128)(2,1)}, bf16[256,512]{1,0:T(8,128)(2,1)}, u32[]{:S(2)}, u32[]{:S(2)}) collective-permute-start(bf16[256,512]{1,0:T(8,128)(2,1)} %fusion.21), channel_id=1, source_target_pairs={{0,4},{4,8},{8,12},{12,16},{16,20},{20,24},{24,28},{1,5},{5,9},{9,... | collective-permute-start | bytes 786440 | tf_op jit(solution)/shard_map/ppermute | solution.py:17
  156.5 2.0 copy-start
  166.4 146.2 %all-gather.14.cloned.1.call-start = ((), (), s32[]{:S(2)}) async-start(), calls=%async_computation.4 | async-start | bytes 9437184 | tf_op jit(solution)/shard_map/all_gather | solution.py:114
Sparse Core Ops, SparseCore 0:
  9.5 83.4 all-gather.9
  95.1 47.2 all-gather.11
  166.5 19.1 all-gather.7
  187.6 124.9 all-gather.13
